TPU v7x, 256 devices: a whole 4x4x8 slice. The times are simulated.
256 devices in a mesh: sp: 16 (over y, x), dp: 16 (over z, core).
Axes of the slice: x: 4, y: 4, z: 8, core: 2. Of those that a mesh axis runs over, the one named last changes fastest.
Arguments:
- tokens: bfloat16 [16, 2048, 2048], P('dp', 'sp'), may hold values from -6 to 6
- query_weight: bfloat16 [2048, 1024], P('dp'), may hold values from -0.125 to 0.125
- key_weight: bfloat16 [2048, 1024], P('dp'), may hold values from -0.125 to 0.125
- value_weight: bfloat16 [2048, 2048], P('dp'), may hold values from -0.125 to 0.125
- output_weight: bfloat16 [2048, 2048], P('dp'), may hold values from -0.125 to 0.125
- log_decay: float32 [2, 16], P(None, 'sp'), may hold values from -0.04 to 0, as said below
Outputs:
- mixed: bfloat16 [16, 2048, 2048], P('dp', 'sp')
Inputs may be any that keep to these rules, and one draw needn't show every extreme that they name: `log_decay`: every entry is negative: the logarithm of a head's decay per position.
All inputs are finite; a program needn't handle non-finite values.
Results may differ from a plain program's by a relative error of at most 0.012.
Values may be sent and summed in bfloat16 or wider, within the bound.
No kernel may reach another device: no remote copies, remote signals or barrier semaphores. Data moves between devices by JAX's collectives and lax.ppermute only.
A program may use at most 128 MiB of HBM per device.

v0:
```python
import jax
import jax.numpy as jnp
from jax import lax
from jax.sharding import PartitionSpec as P

HEADS = 16
DK = 64
DV = 128
BLOCK = 512


def in_order(pieces, dim):
    lengths = list(pieces.shape[1:])
    lengths[dim] *= pieces.shape[0]
    return jnp.moveaxis(pieces, 0, dim).reshape(lengths)


def copy_for_each(shard, axis):
    count = lax.axis_size(axis)
    return lax.all_to_all(
        jnp.broadcast_to(shard[None], (count, *shard.shape)), axis, 0, 0, tiled=True
    )


def gathered_copies(shard, axis, dim):
    return in_order(copy_for_each(shard, axis), dim)


def rotate(values_part, positions):
    half_dim = values_part.shape[-1] // 2
    frequency = 10000.0 ** (-jnp.arange(half_dim, dtype=jnp.float32) / half_dim)
    angles = positions[:, None] * frequency[None, :]
    cosine = jnp.cos(angles)[:, None, :]
    sine_part = jnp.sin(angles)[:, None, :]
    first = values_part[..., :half_dim]
    second = values_part[..., half_dim:]
    return jnp.concatenate(
        [first * cosine - second * sine_part, first * sine_part + second * cosine], axis=-1
    )


def retain(query, key_rows, value_rows, log_rate):
    length, heads, key_dim = query.shape
    value_dim = value_rows.shape[-1]
    count = length // BLOCK
    offsets = jnp.arange(BLOCK, dtype=jnp.float32)
    distance = offsets[:, None] - offsets[None, :]
    decay_inner = jnp.where(
        distance[None] >= 0.0,
        jnp.exp(log_rate[:, None, None] * jnp.maximum(distance, 0.0)[None]),
        0.0,
    )
    decay_query = jnp.exp((offsets[:, None] + 1.0) * log_rate[None, :])[:, :, None]
    decay_key = jnp.exp((BLOCK - 1.0 - offsets)[:, None] * log_rate[None, :])[:, :, None]
    decay_block = jnp.exp(BLOCK * log_rate)[:, None, None]

    def blocks(array):
        return array.reshape(count, BLOCK, heads, array.shape[-1])

    def advance(state, inputs):
        query_block, key_block, value_block = inputs
        inner = (
            jnp.einsum("ihd,jhd->hij", query_block, key_block, preferred_element_type=jnp.float32)
            * decay_inner
        )
        result = jnp.einsum(
            "hij,jhv->ihv",
            inner.astype(jnp.bfloat16),
            value_block,
            preferred_element_type=jnp.float32,
        )
        query_wide = query_block.astype(jnp.float32) * decay_query
        result = result + jnp.einsum("ihd,hdv->ihv", query_wide, state)
        key_wide = key_block.astype(jnp.float32) * decay_key
        state = state * decay_block + jnp.einsum(
            "jhd,jhv->hdv", key_wide, value_block.astype(jnp.float32)
        )
        return (state, result)

    initial = jnp.zeros((heads, key_dim, value_dim), jnp.float32)
    final_state, outputs = lax.scan(
        advance, initial, (blocks(query), blocks(key_rows), blocks(value_rows))
    )
    return outputs.reshape(length, heads, value_dim)


def mechanism(stacked, log_decay):
    length = stacked.shape[0]
    widened = stacked[..., : 2 * DK].astype(jnp.float32)
    positions = jnp.arange(length, dtype=jnp.float32)
    query = rotate(widened[..., :DK], positions).astype(jnp.bfloat16)
    key_rows = rotate(widened[..., DK : 2 * DK], positions).astype(jnp.bfloat16)
    value_rows = stacked[..., 2 * DK :]
    forward = retain(query, key_rows, value_rows, log_decay[0])
    backward = retain(
        jnp.flip(query, 0), jnp.flip(key_rows, 0), jnp.flip(value_rows, 0), log_decay[1]
    )
    combined = forward + jnp.flip(backward, 0)
    average = jnp.mean(combined, axis=-1, keepdims=True)
    centred = combined - average
    variance = jnp.mean(centred * centred, axis=-1, keepdims=True)
    return (centred * lax.rsqrt(variance + 1e-06)).astype(jnp.bfloat16)


def shards(tokens, query_weight, key_weight, value_weight, output_weight, log_decay):
    rows = tokens[0]
    row_count = rows.shape[0]
    local_heads = log_decay.shape[1]
    first_head = lax.axis_index("sp") * local_heads
    own_slices = jnp.concatenate(
        [
            lax.dynamic_slice_in_dim(query_weight, first_head * DK, local_heads * DK, 1),
            lax.dynamic_slice_in_dim(key_weight, first_head * DK, local_heads * DK, 1),
            lax.dynamic_slice_in_dim(value_weight, first_head * DV, local_heads * DV, 1),
        ],
        axis=1,
    )
    own_whole = gathered_copies(own_slices, "dp", 0)
    piece = lax.all_gather(rows, "sp", axis=0, tiled=True)
    count = piece.shape[0]
    product = jnp.dot(piece, own_whole, preferred_element_type=jnp.float32).astype(jnp.bfloat16)
    query_part = product[:, : local_heads * DK].reshape(count, local_heads, DK)
    key_part = product[:, local_heads * DK : 2 * local_heads * DK].reshape(count, local_heads, DK)
    value_part = product[:, 2 * local_heads * DK :].reshape(count, local_heads, DV)
    gathered = jnp.concatenate([query_part, key_part, value_part], axis=2)
    normed = mechanism(gathered, log_decay)
    by_token = lax.all_to_all(normed, "sp", split_axis=0, concat_axis=1, tiled=True).reshape(
        row_count, HEADS * DV
    )
    mixed = jnp.dot(
        by_token,
        lax.all_gather(output_weight, "dp", axis=0, tiled=True),
        preferred_element_type=jnp.float32,
    )
    return mixed.astype(jnp.bfloat16)[None]


def solution(mesh):
    placed = (
        P("dp", "sp", None),
        P("dp", None),
        P("dp", None),
        P("dp", None),
        P("dp", None),
        P(None, "sp"),
    )
    return jax.shard_map(
        shards, mesh=mesh, in_specs=placed, out_specs=P("dp", "sp", None), check_vma=False
    )
```

profile of v0, /device:TPU:32, one launch (start us, length us, event | category | flops | bytes accessed | tf_op | source)
XLA Modules:
  0.0 171.1 jit_solution(11749039148471384118)
XLA Ops:
  6.5 0.7 all-gather.6.cloned.1.call-update
  7.3 0.7 all-gather.4.cloned.1.call-update
  8.0 0.9 constant_dynamic-slice_fusion.1
  9.0 1.1 broadcast_in_dim.18
  10.1 8.6 %all-to-all-start = ((bf16[16,128,256]{2,1,0:T(8,128)(2,1)}), bf16[16,128,256]{2,1,0:T(8,128)(2,1)S(1)}, u32[]{:S(2)}, u32[]{:S(2)}) async-start(bf16[16,128,256]{2,1,0:T(8,128)(2,1)} %broadcast_in_dim.18), calls=%async_computation | async-start | bytes 2097152 | tf_op jit(solution)/shard_map/all_to_all | solution.py:20
  18.7 1.4 fusion.116
  21.5 21.8 %all-to-all-done = bf16[16,128,256]{2,1,0:T(8,128)(2,1)S(1)} async-done(((bf16[16,128,256]{2,1,0:T(8,128)(2,1)}), bf16[16,128,256]{2,1,0:T(8,128)(2,1)S(1)}, u32[]{:S(2)}, u32[]{:S(2)}) %all-to-all-start) | async-done | bytes 1048608 | tf_op jit(solution)/shard_map/all_to_all | solution.py:20
  43.3 45.0 %all-gather.6.cloned.1.call-done = bf16[1,2048,2048]{2,1,0:T(8,128)(2,1)} async-done(((bf16[1,128,2048]{2,1,0:T(8,128)(2,1)}), bf16[1,2048,2048]{2,1,0:T(8,128)(2,1)}) %all-gather.6.cloned.1.call-update) | async-done | bytes 8388624 | tf_op jit(solution)/shard_map/all_gather | solution.py:119
  88.3 5.8 %fusion.109 = bf16[2048,256]{0,1:T(8,128)(2,1)S(1)} fusion(bf16[2048,256]{1,0:T(8,128)(2,1)S(1)} %bitcast.255, bf16[1,2048,2048]{2,1,0:T(8,128)(2,1)} %all-gather.6.cloned.1.call-done), kind=kOutput, calls=%fused_computation.103 | convolution fusion | flops 2148007936 | bytes 10485760 | tf_op jit(solution)/shard_map/dot_general | solution.py:121
  94.1 1.0 copy.52
  95.1 1.6 reverse.3
  96.9 1.2 subtract_convert_fusion
  98.3 1.4 rev.14
  99.7 1.4 rev.13
  101.1 0.8 copy.76
  102.2 17.2 %while.31 = (s32[]{:T(128)}, f32[1,64,128]{2,1,0:T(8,128)S(1)}, f32[4,512,1,128]{3,1,0,2:T(8,128)S(1)}, f32[1,1,1]{2,1,0:T(1,128)}, bf16[4,512,1,64]{1,3,2,0:T(8...) while((s32[]{:T(128)}, f32[1,64,128]{2,1,0:T(8,128)S(1)}, ...), condition=%wide.region_3.4_spmd.clone.clone.clone, body=%wide.region_2.3_spmd.clone.clone.clone.sunk | while | flops 119506944 | bytes 2469500 | solution.py:81
  102.2 2.2 %fusion.158 = f32[128,512]{1,0:T(8,128)S(1)} fusion(f32[]{:T(128)} %get-tuple-element.508, bf16[4,512,1,128]{3,1,2,0:T(8,128)(2,1)S(1)} %get-tuple-element.506, s32[]{:T(128)} %get-tuple-element.491, bf16[4,512,1,64]{1,3,2,0:T(8,128)(2,1)S(1)} %get-tuple-element.507, bf16[4,512,1,64]{1,3,2,0:T(8,128)(2,1)} %get-tuple-element.505), kind=kOutput, calls=%fused_computation.55.clone.1 | convolution fusion | flops 102498304 | bytes 526336 | tf_op jit(solution)/shard_map/while/body/eval_jaxpr/hij,jhv->ihv/dot_general | solution.py:66
  104.4 0.7 multiply_exponential_fusion.7
  105.5 1.0 fusion.157
  106.5 2.2 %fusion.158 = f32[128,512]{1,0:T(8,128)S(1)} fusion(f32[]{:T(128)} %get-tuple-element.508, bf16[4,512,1,128]{3,1,2,0:T(8,128)(2,1)S(1)} %get-tuple-element.506, s32[]{:T(128)} %get-tuple-element.491, bf16[4,512,1,64]{1,3,2,0:T(8,128)(2,1)S(1)} %get-tuple-element.507, bf16[4,512,1,64]{1,3,2,0:T(8,128)(2,1)} %get-tuple-element.505), kind=kOutput, calls=%fused_computation.55.clone.1 | convolution fusion | flops 102498304 | bytes 526336 | tf_op jit(solution)/shard_map/while/body/eval_jaxpr/hij,jhv->ihv/dot_general | solution.py:66
  108.7 0.7 multiply_exponential_fusion.7
  109.8 1.0 fusion.157
  110.9 2.2 %fusion.158 = f32[128,512]{1,0:T(8,128)S(1)} fusion(f32[]{:T(128)} %get-tuple-element.508, bf16[4,512,1,128]{3,1,2,0:T(8,128)(2,1)S(1)} %get-tuple-element.506, s32[]{:T(128)} %get-tuple-element.491, bf16[4,512,1,64]{1,3,2,0:T(8,128)(2,1)S(1)} %get-tuple-element.507, bf16[4,512,1,64]{1,3,2,0:T(8,128)(2,1)} %get-tuple-element.505), kind=kOutput, calls=%fused_computation.55.clone.1 | convolution fusion | flops 102498304 | bytes 526336 | tf_op jit(solution)/shard_map/while/body/eval_jaxpr/hij,jhv->ihv/dot_general | solution.py:66
  113.1 0.7 multiply_exponential_fusion.7
  114.1 1.0 fusion.157
  115.2 2.2 %fusion.158 = f32[128,512]{1,0:T(8,128)S(1)} fusion(f32[]{:T(128)} %get-tuple-element.508, bf16[4,512,1,128]{3,1,2,0:T(8,128)(2,1)S(1)} %get-tuple-element.506, s32[]{:T(128)} %get-tuple-element.491, bf16[4,512,1,64]{1,3,2,0:T(8,128)(2,1)S(1)} %get-tuple-element.507, bf16[4,512,1,64]{1,3,2,0:T(8,128)(2,1)} %get-tuple-element.505), kind=kOutput, calls=%fused_computation.55.clone.1 | convolution fusion | flops 102498304 | bytes 526336 | tf_op jit(solution)/shard_map/while/body/eval_jaxpr/hij,jhv->ihv/dot_general | solution.py:66
  117.4 0.7 multiply_exponential_fusion.7
  118.5 1.0 fusion.157
  119.9 0.7 pad_maximum_fusion
  120.7 17.5 %while.30 = (s32[]{:T(128)}, f32[1,64,128]{2,1,0:T(8,128)S(1)}, f32[4,512,1,128]{3,1,0,2:T(8,128)S(1)}, f32[1,1,1]{2,1,0:T(1,128)}, bf16[4,512,1,64]{1,3,2,0:T(8...) while((s32[]{:T(128)}, f32[1,64,128]{2,1,0:T(8,128)S(1)}, ...), condition=%wide.region_1.2_spmd.clone.clone.clone, body=%wide.region_0.1_spmd.clone.clone.clone.sunk | while | flops 119506944 | bytes 2469500 | solution.py:81
  120.7 2.2 %fusion.148 = f32[128,512]{1,0:T(8,128)S(1)} fusion(f32[]{:T(128)} %get-tuple-element.538, bf16[4,512,1,128]{3,1,2,0:T(8,128)(2,1)} %get-tuple-element.536, s32[]{:T(128)} %get-tuple-element.521, bf16[4,512,1,64]{1,3,2,0:T(8,128)(2,1)S(1)} %get-tuple-element.537, bf16[4,512,1,64]{1,3,2,0:T(8,128)(2,1)} %get-tuple-element.535), kind=kOutput, calls=%fused_computation.8.clone.1 | convolution fusion | flops 102498304 | bytes 526336 | tf_op jit(solution)/shard_map/while/body/eval_jaxpr/hij,jhv->ihv/dot_general | solution.py:66
  122.9 0.6 multiply_exponential_fusion.6
  124.0 1.1 fusion.147
  125.1 2.2 %fusion.148 = f32[128,512]{1,0:T(8,128)S(1)} fusion(f32[]{:T(128)} %get-tuple-element.538, bf16[4,512,1,128]{3,1,2,0:T(8,128)(2,1)} %get-tuple-element.536, s32[]{:T(128)} %get-tuple-element.521, bf16[4,512,1,64]{1,3,2,0:T(8,128)(2,1)S(1)} %get-tuple-element.537, bf16[4,512,1,64]{1,3,2,0:T(8,128)(2,1)} %get-tuple-element.535), kind=kOutput, calls=%fused_computation.8.clone.1 | convolution fusion | flops 102498304 | bytes 526336 | tf_op jit(solution)/shard_map/while/body/eval_jaxpr/hij,jhv->ihv/dot_general | solution.py:66
  127.3 0.6 multiply_exponential_fusion.6
  128.3 1.1 fusion.147
  129.4 2.2 %fusion.148 = f32[128,512]{1,0:T(8,128)S(1)} fusion(f32[]{:T(128)} %get-tuple-element.538, bf16[4,512,1,128]{3,1,2,0:T(8,128)(2,1)} %get-tuple-element.536, s32[]{:T(128)} %get-tuple-element.521, bf16[4,512,1,64]{1,3,2,0:T(8,128)(2,1)S(1)} %get-tuple-element.537, bf16[4,512,1,64]{1,3,2,0:T(8,128)(2,1)} %get-tuple-element.535), kind=kOutput, calls=%fused_computation.8.clone.1 | convolution fusion | flops 102498304 | bytes 526336 | tf_op jit(solution)/shard_map/while/body/eval_jaxpr/hij,jhv->ihv/dot_general | solution.py:66
  131.7 0.6 multiply_exponential_fusion.6
  132.7 1.1 fusion.147
  133.8 2.2 %fusion.148 = f32[128,512]{1,0:T(8,128)S(1)} fusion(f32[]{:T(128)} %get-tuple-element.538, bf16[4,512,1,128]{3,1,2,0:T(8,128)(2,1)} %get-tuple-element.536, s32[]{:T(128)} %get-tuple-element.521, bf16[4,512,1,64]{1,3,2,0:T(8,128)(2,1)S(1)} %get-tuple-element.537, bf16[4,512,1,64]{1,3,2,0:T(8,128)(2,1)} %get-tuple-element.535), kind=kOutput, calls=%fused_computation.8.clone.1 | convolution fusion | flops 102498304 | bytes 526336 | tf_op jit(solution)/shard_map/while/body/eval_jaxpr/hij,jhv->ihv/dot_general | solution.py:66
  136.0 0.6 multiply_exponential_fusion.6
  137.1 1.1 fusion.147
  138.5 0.6 multiply_reduce_fusion
  139.2 0.6 multiply_convert_fusion
  140.3 1.0 reduce.2
  141.5 16.4 %all_to_all.20 = bf16[16,2,8192]{2,1,0:T(2,128)(2,1)S(1)} all-to-all(bf16[16,2,8192]{2,1,0:T(2,128)(2,1)S(1)} %reshape.742), channel_id=1, replica_groups=mesh['sp'=16,'dp'=16] {'sp'}, dimensions={0} | all-to-all | bytes 1048576 | tf_op jit(solution)/shard_map/all_to_all | solution.py:127
  157.9 0.5 reshape.743
  158.8 5.5 %fusion.112 = bf16[1,128,2048]{2,1,0:T(8,128)(2,1)} fusion(bf16[128,2048]{0,1:T(8,128)(2,1)S(1)} %bitcast.246, bf16[2048,2048]{1,0:T(8,128)(2,1)} %all-gather.4.cloned.1.call-done), kind=kOutput, calls=%fused_computation.105 | convolution fusion | flops 1074003968 | bytes 9437184 | tf_op jit(solution)/shard_map/dot_general | solution.py:130
  (56 shorter events, 5.6 us)
Async XLA Ops:
  6.5 1.5 copy-start
  6.5 81.7 %all-gather.6.cloned.1.call-start = ((), (), s32[]{:S(2)}) async-start(), calls=%async_computation.3 | async-start | bytes 8912896 | tf_op jit(solution)/shard_map/all_gather | solution.py:119
  7.3 151.5 %all-gather.4.cloned.1.call-start = ((), (), s32[]{:S(2)}) async-start(), calls=%async_computation.2 | async-start | bytes 8912896 | tf_op jit(solution)/shard_map/all_gather | solution.py:132
  10.1 33.2 %all-to-all-start = ((bf16[16,128,256]{2,1,0:T(8,128)(2,1)}), bf16[16,128,256]{2,1,0:T(8,128)(2,1)S(1)}, u32[]{:S(2)}, u32[]{:S(2)}) async-start(bf16[16,128,256]{2,1,0:T(8,128)(2,1)} %broadcast_in_dim.18), calls=%async_computation | async-start | bytes 2097152 | tf_op jit(solution)/shard_map/all_to_all | solution.py:20
Sparse Core Ops, SparseCore 0:
  9.8 78.4 all-gather.5
  90.1 53.8 all-gather.3
where the time goes:
time: 172 us; the launch traced here: 171 us
  waiting for transfers between devices  68.2 us (40%)
  matrix products  39 us (23%)
  blocking collectives  16.4 us (10%)
  between operations  15 us (9%)
  local copies, waits for them, and re-layouts  13.2 us (8%)
  other arithmetic  10.2 us (6%)
  starting transfers between devices  8.63 us (5%)
    all_gather x1, waiting for transfers between devices, shards(): piece = lax.all_gather(rows, 'sp', axis=0, tiled=True)  45 us
    all_to_all x1, waiting for transfers between devices, copy_for_each(): lax.all_to_all(jnp.broadcast_to(shard[None], (count, *shard.shape)), axis...  21.8 us
    dot_general x8, matrix products, advance(): jnp.einsum('hij,jhv->ihv', inner.astype(jnp.bfloat16), value_block, prefe...  17.5 us
    all_to_all x1, blocking collectives, shards(): lax.all_to_all(normed, 'sp', split_axis=0, concat_axis=1, tiled=True)  16.4 us
    all_to_all x1, starting transfers between devices, copy_for_each(): lax.all_to_all(jnp.broadcast_to(shard[None], (count, *shard.shape)), axis...  8.59 us
    dot_general x8, matrix products, advance(): jnp.einsum('jhd,jhv->hdv', key_wide, value_block.astype(jnp.float32))  8.43 us
    dot_general x1, matrix products, shards(): jnp.dot(piece, own_whole, preferred_element_type=jnp.float32)  5.77 us
    dot_general x1, matrix products, shards(): jnp.dot(by_token, lax.all_gather(output_weight, 'dp', axis=0, tiled=True)...  5.47 us
  transfers between devices with their start and end apart: 3, of which 2 were waited for; matrix products, arithmetic and copies ran while one was open for 33% of the time, Pallas kernels for 0%

commit v1 on v0

--- a/solution.py
+++ b/solution.py
@@ -1,3 +1,4 @@
+import functools
 import jax
 import jax.numpy as jnp
 from jax import lax
@@ -7,6 +8,18 @@
 DK = 64
 DV = 128
 BLOCK = 512
+
+
+def lead_series_all(mine_x, row_axis):
+    return jnp.concatenate(
+        lax.all_to_all(
+            jnp.stack(jnp.split(mine_x, lax.axis_size(row_axis), axis=0), 0), row_axis, 0, 0
+        ),
+        axis=1,
+    )
+
+
+roads_apply = functools.partial(lead_series_all, row_axis="sp")
 
 
 def in_order(pieces, dim):
@@ -124,9 +137,7 @@
     value_part = product[:, 2 * local_heads * DK :].reshape(count, local_heads, DV)
     gathered = jnp.concatenate([query_part, key_part, value_part], axis=2)
     normed = mechanism(gathered, log_decay)
-    by_token = lax.all_to_all(normed, "sp", split_axis=0, concat_axis=1, tiled=True).reshape(
-        row_count, HEADS * DV
-    )
+    by_token = roads_apply(normed).reshape(row_count, HEADS * DV)
     mixed = jnp.dot(
         by_token,
         lax.all_gather(output_weight, "dp", axis=0, tiled=True),

time: 172 us -> 170 us (0.988)
  transfers between devices with their start and end apart: 3 -> 3, of which waited for: 2 -> 2; matrix products, arithmetic and copies ran while one was open for 33% -> 32% of each run, Pallas kernels for 0% -> 0%
where the time goes in v1:
time: 170 us; the launch traced here: 169 us
  waiting for transfers between devices  68.4 us (40%)
  matrix products  38.8 us (23%)
  blocking collectives  16.4 us (10%)
  between operations  15.1 us (9%)
  local copies, waits for them, and re-layouts  12 us (7%)
  other arithmetic  8.94 us (5%)
  starting transfers between devices  8.63 us (5%)
    all_gather x1, waiting for transfers between devices, shards(): piece = lax.all_gather(rows, 'sp', axis=0, tiled=True)  45 us
    all_to_all x1, waiting for transfers between devices, copy_for_each(): lax.all_to_all(jnp.broadcast_to(shard[None], (count, *shard.shape)), axis...  21.9 us
    dot_general x8, matrix products, advance(): jnp.einsum('hij,jhv->ihv', inner.astype(jnp.bfloat16), value_block, prefe...  17.3 us
    all_to_all x1, blocking collectives, lead_series_all(): lax.all_to_all(jnp.stack(jnp.split(mine_x, lax.axis_size(row_axis), axis=...  16.4 us
    all_to_all x1, starting transfers between devices, copy_for_each(): lax.all_to_all(jnp.broadcast_to(shard[None], (count, *shard.shape)), axis...  8.59 us
    dot_general x8, matrix products, advance(): jnp.einsum('jhd,jhv->hdv', key_wide, value_block.astype(jnp.float32))  8.46 us
    dot_general x1, matrix products, shards(): jnp.dot(piece, own_whole, preferred_element_type=jnp.float32)  5.77 us
    dot_general x1, matrix products, shards(): jnp.dot(by_token, lax.all_gather(output_weight, 'dp', axis=0, tiled=True)...  5.46 us
  transfers between devices with their start and end apart: 3, of which 2 were waited for; matrix products, arithmetic and copies ran while one was open for 32% of the time, Pallas kernels for 0%

profile of v1, /device:TPU:32, one launch (start us, length us, event | category | flops | bytes accessed | tf_op | source)
XLA Modules:
  0.0 168.7 jit_solution(14280036012243845060)
XLA Ops:
  6.5 0.7 all-gather.6.cloned.1.call-update
  7.3 0.7 all-gather.4.cloned.1.call-update
  8.0 0.9 constant_dynamic-slice_fusion.1
  9.0 1.1 broadcast_in_dim.18
  10.1 8.6 %all-to-all-start = ((bf16[16,128,256]{2,1,0:T(8,128)(2,1)}), bf16[16,128,256]{2,1,0:T(8,128)(2,1)S(1)}, u32[]{:S(2)}, u32[]{:S(2)}) async-start(bf16[16,128,256]{2,1,0:T(8,128)(2,1)} %broadcast_in_dim.18), calls=%async_computation | async-start | bytes 2097152 | tf_op jit(solution)/shard_map/all_to_all | solution.py:33
  18.7 1.3 fusion.116
  21.4 21.9 %all-to-all-done = bf16[16,128,256]{2,1,0:T(8,128)(2,1)S(1)} async-done(((bf16[16,128,256]{2,1,0:T(8,128)(2,1)}), bf16[16,128,256]{2,1,0:T(8,128)(2,1)S(1)}, u32[]{:S(2)}, u32[]{:S(2)}) %all-to-all-start) | async-done | bytes 1048608 | tf_op jit(solution)/shard_map/all_to_all | solution.py:33
  43.3 45.0 %all-gather.6.cloned.1.call-done = bf16[1,2048,2048]{2,1,0:T(8,128)(2,1)} async-done(((bf16[1,128,2048]{2,1,0:T(8,128)(2,1)}), bf16[1,2048,2048]{2,1,0:T(8,128)(2,1)}) %all-gather.6.cloned.1.call-update) | async-done | bytes 8388624 | tf_op jit(solution)/shard_map/all_gather | solution.py:132
  88.3 5.8 %fusion.109 = bf16[2048,256]{0,1:T(8,128)(2,1)S(1)} fusion(bf16[2048,256]{1,0:T(8,128)(2,1)S(1)} %bitcast.317, bf16[1,2048,2048]{2,1,0:T(8,128)(2,1)} %all-gather.6.cloned.1.call-done), kind=kOutput, calls=%fused_computation.103 | convolution fusion | flops 2148007936 | bytes 10485760 | tf_op jit(solution)/shard_map/dot_general | solution.py:134
  94.1 1.0 copy.51
  95.1 1.6 reverse.3
  96.9 1.2 subtract_convert_fusion
  98.3 1.4 rev.14
  99.7 1.4 rev.13
  101.1 0.8 copy.74
  102.2 16.3 %while.31 = (s32[]{:T(128)}, f32[1,64,128]{2,1,0:T(8,128)S(1)}, f32[4,512,1,128]{3,1,0,2:T(8,128)S(1)}, f32[1,1,1]{2,1,0:T(1,128)}, bf16[4,512,1,64]{1,3,2,0:T(8...) while((s32[]{:T(128)}, f32[1,64,128]{2,1,0:T(8,128)S(1)}, ...), condition=%wide.region_3.4_spmd.clone.clone.clone, body=%wide.region_2.3_spmd.clone.clone.clone.sunk | while | flops 119506944 | bytes 2469500 | solution.py:94
  102.2 2.1 %fusion.158 = f32[128,512]{1,0:T(8,128)S(1)} fusion(f32[]{:T(128)} %get-tuple-element.492, bf16[4,512,1,128]{3,1,2,0:T(8,128)(2,1)S(1)} %get-tuple-element.490, s32[]{:T(128)} %get-tuple-element.475, bf16[4,512,1,64]{1,3,2,0:T(8,128)(2,1)S(1)} %get-tuple-element.491, bf16[4,512,1,64]{1,3,2,0:T(8,128)(2,1)} %get-tuple-element.489), kind=kOutput, calls=%fused_computation.55.clone.1 | convolution fusion | flops 102498304 | bytes 526336 | tf_op jit(solution)/shard_map/while/body/eval_jaxpr/hij,jhv->ihv/dot_general | solution.py:79
  104.3 0.6 multiply_exponential_fusion.7
  105.3 1.0 fusion.157
  106.3 2.1 %fusion.158 = f32[128,512]{1,0:T(8,128)S(1)} fusion(f32[]{:T(128)} %get-tuple-element.492, bf16[4,512,1,128]{3,1,2,0:T(8,128)(2,1)S(1)} %get-tuple-element.490, s32[]{:T(128)} %get-tuple-element.475, bf16[4,512,1,64]{1,3,2,0:T(8,128)(2,1)S(1)} %get-tuple-element.491, bf16[4,512,1,64]{1,3,2,0:T(8,128)(2,1)} %get-tuple-element.489), kind=kOutput, calls=%fused_computation.55.clone.1 | convolution fusion | flops 102498304 | bytes 526336 | tf_op jit(solution)/shard_map/while/body/eval_jaxpr/hij,jhv->ihv/dot_general | solution.py:79
  108.4 0.6 multiply_exponential_fusion.7
  109.4 1.0 fusion.157
  110.4 2.1 %fusion.158 = f32[128,512]{1,0:T(8,128)S(1)} fusion(f32[]{:T(128)} %get-tuple-element.492, bf16[4,512,1,128]{3,1,2,0:T(8,128)(2,1)S(1)} %get-tuple-element.490, s32[]{:T(128)} %get-tuple-element.475, bf16[4,512,1,64]{1,3,2,0:T(8,128)(2,1)S(1)} %get-tuple-element.491, bf16[4,512,1,64]{1,3,2,0:T(8,128)(2,1)} %get-tuple-element.489), kind=kOutput, calls=%fused_computation.55.clone.1 | convolution fusion | flops 102498304 | bytes 526336 | tf_op jit(solution)/shard_map/while/body/eval_jaxpr/hij,jhv->ihv/dot_general | solution.py:79
  112.5 0.6 multiply_exponential_fusion.7
  113.5 1.0 fusion.157
  114.5 2.1 %fusion.158 = f32[128,512]{1,0:T(8,128)S(1)} fusion(f32[]{:T(128)} %get-tuple-element.492, bf16[4,512,1,128]{3,1,2,0:T(8,128)(2,1)S(1)} %get-tuple-element.490, s32[]{:T(128)} %get-tuple-element.475, bf16[4,512,1,64]{1,3,2,0:T(8,128)(2,1)S(1)} %get-tuple-element.491, bf16[4,512,1,64]{1,3,2,0:T(8,128)(2,1)} %get-tuple-element.489), kind=kOutput, calls=%fused_computation.55.clone.1 | convolution fusion | flops 102498304 | bytes 526336 | tf_op jit(solution)/shard_map/while/body/eval_jaxpr/hij,jhv->ihv/dot_general | solution.py:79
  116.6 0.6 multiply_exponential_fusion.7
  117.6 1.0 fusion.157
  118.6 0.4 rev.15
  119.0 0.7 pad_maximum_fusion
  119.8 17.9 %while.30 = (s32[]{:T(128)}, f32[1,64,128]{2,1,0:T(8,128)S(1)}, f32[4,512,1,128]{3,1,0,2:T(8,128)S(1)}, f32[1,1,1]{2,1,0:T(1,128)}, bf16[4,512,1,64]{1,3,2,0:T(8...) while((s32[]{:T(128)}, f32[1,64,128]{2,1,0:T(8,128)S(1)}, ...), condition=%wide.region_1.2_spmd.clone.clone.clone, body=%wide.region_0.1_spmd.clone.clone.clone.sunk | while | flops 119506944 | bytes 2469500 | solution.py:94
  119.8 2.3 %fusion.148 = f32[128,512]{1,0:T(8,128)S(1)} fusion(f32[]{:T(128)} %get-tuple-element.522, bf16[4,512,1,128]{3,1,2,0:T(8,128)(2,1)} %get-tuple-element.520, s32[]{:T(128)} %get-tuple-element.505, bf16[4,512,1,64]{1,3,2,0:T(8,128)(2,1)S(1)} %get-tuple-element.521, bf16[4,512,1,64]{1,3,2,0:T(8,128)(2,1)} %get-tuple-element.519), kind=kOutput, calls=%fused_computation.8.clone.1 | convolution fusion | flops 102498304 | bytes 526336 | tf_op jit(solution)/shard_map/while/body/eval_jaxpr/hij,jhv->ihv/dot_general | solution.py:79
  122.1 0.7 multiply_exponential_fusion.6
  123.2 1.1 fusion.147
  124.3 2.3 %fusion.148 = f32[128,512]{1,0:T(8,128)S(1)} fusion(f32[]{:T(128)} %get-tuple-element.522, bf16[4,512,1,128]{3,1,2,0:T(8,128)(2,1)} %get-tuple-element.520, s32[]{:T(128)} %get-tuple-element.505, bf16[4,512,1,64]{1,3,2,0:T(8,128)(2,1)S(1)} %get-tuple-element.521, bf16[4,512,1,64]{1,3,2,0:T(8,128)(2,1)} %get-tuple-element.519), kind=kOutput, calls=%fused_computation.8.clone.1 | convolution fusion | flops 102498304 | bytes 526336 | tf_op jit(solution)/shard_map/while/body/eval_jaxpr/hij,jhv->ihv/dot_general | solution.py:79
  126.6 0.7 multiply_exponential_fusion.6
  127.7 1.1 fusion.147
  128.8 2.3 %fusion.148 = f32[128,512]{1,0:T(8,128)S(1)} fusion(f32[]{:T(128)} %get-tuple-element.522, bf16[4,512,1,128]{3,1,2,0:T(8,128)(2,1)} %get-tuple-element.520, s32[]{:T(128)} %get-tuple-element.505, bf16[4,512,1,64]{1,3,2,0:T(8,128)(2,1)S(1)} %get-tuple-element.521, bf16[4,512,1,64]{1,3,2,0:T(8,128)(2,1)} %get-tuple-element.519), kind=kOutput, calls=%fused_computation.8.clone.1 | convolution fusion | flops 102498304 | bytes 526336 | tf_op jit(solution)/shard_map/while/body/eval_jaxpr/hij,jhv->ihv/dot_general | solution.py:79
  131.1 0.7 multiply_exponential_fusion.6
  132.2 1.1 fusion.147
  133.3 2.3 %fusion.148 = f32[128,512]{1,0:T(8,128)S(1)} fusion(f32[]{:T(128)} %get-tuple-element.522, bf16[4,512,1,128]{3,1,2,0:T(8,128)(2,1)} %get-tuple-element.520, s32[]{:T(128)} %get-tuple-element.505, bf16[4,512,1,64]{1,3,2,0:T(8,128)(2,1)S(1)} %get-tuple-element.521, bf16[4,512,1,64]{1,3,2,0:T(8,128)(2,1)} %get-tuple-element.519), kind=kOutput, calls=%fused_computation.8.clone.1 | convolution fusion | flops 102498304 | bytes 526336 | tf_op jit(solution)/shard_map/while/body/eval_jaxpr/hij,jhv->ihv/dot_general | solution.py:79
  135.6 0.7 multiply_exponential_fusion.6
  136.7 1.1 fusion.147
  137.8 0.3 fusion.115
  138.1 0.6 multiply_reduce_fusion
  138.8 0.6 multiply_convert_fusion
  139.6 16.4 %all_to_all.10 = bf16[16,128,1,128]{3,1,2,0:T(8,128)(2,1)S(1)} all-to-all(bf16[16,128,1,128]{3,1,2,0:T(8,128)(2,1)S(1)} %constant_dynamic-update-slice_fusion.2), channel_id=1, replica_groups=mesh['sp'=16,'dp'=16] {'sp'}, dimensions={0} | all-to-all | bytes 1048576 | tf_op jit(solution)/shard_map/all_to_all | solution.py:15
  156.4 5.5 %fusion.112 = bf16[1,128,2048]{2,1,0:T(8,128)(2,1)} fusion(bf16[128,2048]{0,1:T(8,128)(2,1)S(1)} %bitcast.308, bf16[2048,2048]{1,0:T(8,128)(2,1)} %all-gather.4.cloned.1.call-done), kind=kOutput, calls=%fused_computation.105 | convolution fusion | flops 1074003968 | bytes 9437184 | tf_op jit(solution)/shard_map/dot_general | solution.py:141
  (67 shorter events, 4.3 us)
Async XLA Ops:
  6.5 1.5 copy-start
  6.5 81.7 %all-gather.6.cloned.1.call-start = ((), (), s32[]{:S(2)}) async-start(), calls=%async_computation.3 | async-start | bytes 8912896 | tf_op jit(solution)/shard_map/all_gather | solution.py:132
  7.3 149.1 %all-gather.4.cloned.1.call-start = ((), (), s32[]{:S(2)}) async-start(), calls=%async_computation.2 | async-start | bytes 8912896 | tf_op jit(solution)/shard_map/all_gather | solution.py:143
  10.1 33.2 %all-to-all-start = ((bf16[16,128,256]{2,1,0:T(8,128)(2,1)}), bf16[16,128,256]{2,1,0:T(8,128)(2,1)S(1)}, u32[]{:S(2)}, u32[]{:S(2)}) async-start(bf16[16,128,256]{2,1,0:T(8,128)(2,1)} %broadcast_in_dim.18), calls=%async_computation | async-start | bytes 2097152 | tf_op jit(solution)/shard_map/all_to_all | solution.py:33
Sparse Core Ops, SparseCore 0:
  9.8 78.4 all-gather.5
  90.1 53.8 all-gather.3
